TPU v7x, 512 devices: a whole 4x8x8 slice. The times are simulated.
512 devices in a mesh: sp: 128 (over z, y, core), tp: 4 (over x).
Axes of the slice: x: 4, y: 8, z: 8, core: 2. Of those that a mesh axis runs over, the one named last changes fastest.
Arguments:
- tokens: bfloat16 [16384, 2048], P(('sp', 'tp')), may hold values from -6 to 6
- doc_lengths: int32 [16], replicated, may hold values from 1 to 10240, 16384 in all
- query_down: bfloat16 [2048, 512], replicated, may hold values from -0.125 to 0.125
- latent_down: bfloat16 [2048, 256], replicated, may hold values from -0.125 to 0.125
- rope_down: bfloat16 [2048, 32], replicated, may hold values from -0.125 to 0.125
- query_latent_gain: float32 [512], replicated, may hold values from 0.1 to 1.9
- latent_gain: float32 [256], replicated, may hold values from 0.1 to 1.9
- query_up: bfloat16 [512, 768], P(None, 'tp'), may hold values from -0.25 to 0.25
- key_up: bfloat16 [256, 512], P(None, 'tp'), may hold values from -0.375 to 0.375
- value_up: bfloat16 [256, 512], P(None, 'tp'), may hold values from -0.375 to 0.375
- query_gain: float32 [96], replicated, may hold values from 0.5 to 15
- key_gain: float32 [96], replicated, may hold values from 0.5 to 15
- output_gain: float32 [512], replicated, may hold values from 0.1 to 1.9
- output_weight: bfloat16 [512, 2048], P(None, 'tp'), may hold values from -0.25 to 0.25
Outputs:
- layer_output: bfloat16 [16384, 2048], P('sp', 'tp')
- log_totals: float32 [8, 16384], P('tp', 'sp')
Inputs may be any that keep to these rules, and one draw needn't show every extreme that they name: `doc_lengths`: the lengths sum to 16384; the longest is exactly 10240.
All inputs are finite; a program needn't handle non-finite values.
Results may differ from a plain program's by a relative error of at most 0.019.
The roundings to bfloat16 on the way count: a program that leaves them out, or rounds other values in their place, can miss the bound.
Values may be sent and summed in bfloat16 or wider, within the bound.
No kernel may reach another device: no remote copies, remote signals or barrier semaphores. Data moves between devices by JAX's collectives and lax.ppermute only.
A program may use at most 64 MiB of HBM per device.

v0:
```python
import math

import jax
import jax.numpy as jnp
from jax import lax
from jax.experimental import pallas as pl
from jax.experimental.pallas import tpu as pltpu
from jax.sharding import Mesh, PartitionSpec as P


NOPE = 64
ROPE = 32
VD = 64
HW = NOPE + ROPE
KV = HW + VD
HALF = ROPE // 2

EPS = 1e-06
THETA = 10000.0
NEG = -1e30
START = -1e29
ZS, YS, CS, XS = 8, 8, 2, 4
ROWS = 128
QB = 256
KB = 256
MSG = VD + 16
SCALE = HW ** (-0.5)
SCALE2 = SCALE * math.log2(math.e)

f32 = jnp.float32
bf16 = jnp.bfloat16


def norm_rows(matrix, scaling):
    mean_square = jnp.mean(matrix * matrix, axis=-1, keepdims=True)
    return matrix * lax.rsqrt(mean_square + EPS) * scaling


def spread(value, axes):
    count = 1
    for a in axes:
        count *= lax.axis_size(a)
    copies = jnp.broadcast_to(value, (count, *value.shape))
    return lax.all_to_all(copies, axes, split_axis=0, concat_axis=0, tiled=True)


def rotated(a, b, cosine, sine):
    return a * cosine - b * sine, b * cosine + a * sine


def kv_kernel(lat_ref, rope_ref, key_up_ref, value_up_ref, gain_ref, cos_ref, sin_ref, out_ref):
    lat = lat_ref[...]
    plain = lax.dot_general(
        key_up_ref[...], lat, (((0,), (1,)), ((), ())), preferred_element_type=f32
    )
    value = lax.dot_general(
        value_up_ref[...], lat, (((0,), (1,)), ((), ())), preferred_element_type=f32
    ).astype(bf16)
    shared = rope_ref[...].astype(f32)
    shared = jnp.transpose(jnp.concatenate([shared, jnp.zeros((ROWS, 128 - ROPE), f32)], axis=1))
    shared = shared[:ROPE]
    shared_square = jnp.sum(shared * shared, axis=0, keepdims=True)
    gain = gain_ref[...]
    cosine, sine = cos_ref[...], sin_ref[...]
    for c in range(CS):
        mine = plain[c * NOPE : (c + 1) * NOPE]
        square = (jnp.sum(mine * mine, axis=0, keepdims=True) + shared_square) * (1.0 / HW)
        scale = lax.rsqrt(square + EPS)
        top = mine * scale * gain[:NOPE]
        low = shared * scale * gain[NOPE:]
        a, b = rotated(low[:HALF], low[HALF:], cosine, sine)
        block = jnp.concatenate([top, a, b], axis=0).astype(bf16)
        for z in range(ZS):
            out_ref[z * CS + c, :HW, :] = block
            out_ref[z * CS + c, HW:, :] = value[c * VD : (c + 1) * VD]


def q_kernel(lat_ref, query_up_ref, gain_ref, cos_ref, sin_ref, out_ref):
    raw = lax.dot_general(
        query_up_ref[...], lat_ref[...], (((0,), (1,)), ((), ())), preferred_element_type=f32
    )
    gain = gain_ref[...]
    cosine, sine = cos_ref[...], sin_ref[...]
    for c in range(CS):
        mine = raw[c * HW : (c + 1) * HW]
        square = jnp.sum(mine * mine, axis=0, keepdims=True) * (1.0 / HW)
        mine = mine * lax.rsqrt(square + EPS) * gain
        a, b = rotated(mine[NOPE : NOPE + HALF], mine[NOPE + HALF :], cosine, sine)
        block = jnp.concatenate([mine[:NOPE], a, b], axis=0).astype(bf16)
        out_ref[c * HW : (c + 1) * HW, :] = block


def split_rows(value, width):
    high = value.astype(bf16).astype(f32)
    rest = value - high
    middle = rest.astype(bf16).astype(f32)
    low = rest - middle
    row = lax.broadcasted_iota(jnp.int32, (16, width), 0)
    zero = jnp.zeros((16, width), f32)
    both = jnp.where(row == 0, high, jnp.where(row == 1, middle, jnp.where(row == 2, low, zero)))
    return both.astype(bf16)


def joined_rows(rows):
    rows = rows.astype(f32)
    return (rows[0:1] + rows[1:2]) + rows[2:3]


SUB = 2
DOCS = 16
PAD = 128 - HW


def ends_of(lengths):
    ends = [lengths[0]]
    for i in range(1, DOCS):
        ends.append(ends[-1] + lengths[i])
    return ends


def doc_of(place, ends):
    doc = (place >= ends[0]).astype(jnp.int32)
    for end in ends[1:]:
        doc = doc + (place >= end).astype(jnp.int32)
    return doc


def attend_kernel(lengths, q_ref, kv_ref, out_ref, k_s, q_s, m_s, l_s, acc_s):
    ends = ends_of(lengths)
    query_base = lax.axis_index("z") * (YS * QB)
    key_base = lax.axis_index("y") * KB
    mine = pl.ds(pl.multiple_of(lax.axis_index("c") * HW, HW), HW)
    row = lax.broadcasted_iota(jnp.int32, (YS, QB), 0)
    lane = lax.broadcasted_iota(jnp.int32, (YS, QB), 1)
    query_doc = doc_of(query_base + row * QB + lane, ends)
    key_doc = doc_of(key_base + row * (YS * QB) + lane, ends)
    index = lax.broadcasted_iota(jnp.int32, (PAD, QB), 0)
    for i in range(ZS * CS):
        half = slice((i % CS) * ROWS, (i % CS + 1) * ROWS)
        same = index[:, half] == key_doc[i // CS : i // CS + 1, half]
        part = jnp.where(same, 1.0, 0.0).astype(bf16)
        k_s[i * ROWS : (i + 1) * ROWS, :] = jnp.transpose(
            jnp.concatenate([kv_ref[i, :HW, :], part], axis=0)
        )
    for i in range(YS):
        q_s[i, :HW, :] = jnp.concatenate(
            [q_ref[2 * i, mine, :], q_ref[2 * i + 1, mine, :]], axis=1
        )
        other = (index != query_doc[i : i + 1]) & (index < DOCS)
        q_s[i, HW:, :] = jnp.where(other, NEG, 0.0).astype(bf16)
    m_s[...] = jnp.full(m_s.shape, START, f32)
    l_s[...] = jnp.zeros(l_s.shape, f32)
    acc_s[...] = jnp.zeros(acc_s.shape, f32)

    def block(t, j):
        keys = k_s[pl.ds(j * KB, KB), :]
        values = jnp.concatenate([kv_ref[2 * j, HW:, :], kv_ref[2 * j + 1, HW:, :]], axis=1)
        for s in range(SUB):
            at = t * SUB + s
            scores = jnp.dot(keys, q_s[at], preferred_element_type=f32)
            before = m_s[at]
            now = jnp.maximum(before, jnp.max(scores, axis=0, keepdims=True))
            weights = jnp.exp2((scores - now) * SCALE2)
            rescale = jnp.exp2((before - now) * SCALE2)
            m_s[at] = now
            l_s[at] = l_s[at] * rescale + jnp.sum(weights, axis=0, keepdims=True)
            acc_s[at] = acc_s[at] * rescale + jnp.dot(
                values, weights.astype(bf16), preferred_element_type=f32
            )

    def query_step(t, _):
        begin = query_base + t * (SUB * QB)
        first = doc_of(begin, ends)
        last = doc_of(begin + (SUB * QB - 1), ends)

        def key_step(j, _):
            start = key_base + j * (YS * QB)
            least = doc_of(start, ends)
            most = doc_of(start + (KB - 1), ends)

            @pl.when((least <= last) & (most >= first))
            def _():
                block(t, j)

            return 0

        return lax.fori_loop(0, ZS, key_step, 0)

    lax.fori_loop(0, YS // SUB, query_step, 0)
    for i in range(YS):
        total = l_s[i]
        some = total > 0.0
        safe = jnp.where(some, total, 1.0)
        logs = jnp.where(some, m_s[i] * SCALE + jnp.log(safe), NEG)
        out_ref[i, :VD, :] = (acc_s[i] / safe).astype(bf16)
        out_ref[i, VD:, :] = split_rows(logs, QB)


def combine_kernel(in_ref, out_ref):
    logs = [joined_rows(in_ref[i, VD:, :]) for i in range(YS)]
    top = logs[0]
    for v in logs[1:]:
        top = jnp.maximum(top, v)
    total = jnp.zeros((1, QB), f32)
    mixed = jnp.zeros((VD, QB), f32)
    for i in range(YS):
        w = jnp.exp(logs[i] - top)
        total = total + w
        mixed = mixed + w * in_ref[i, :VD, :].astype(f32)
    head = (mixed / total).astype(bf16)
    tail = split_rows(top + jnp.log(total), QB)
    for c in range(CS):
        for x in range(XS):
            out_ref[c * XS + x, :VD, :] = head[:, c * ROWS : (c + 1) * ROWS]
            out_ref[c * XS + x, VD:, :] = tail[:, c * ROWS : (c + 1) * ROWS]


def output_kernel(x_at, in_ref, gain_ref, weight_ref, out_ref, log_ref):
    heads = []
    for x in range(XS):
        for c in range(CS):
            heads.append(in_ref[c * XS + x, :VD, :].astype(f32))
    joined = jnp.concatenate(heads, axis=0)
    square = jnp.sum(joined * joined, axis=0, keepdims=True) * (1.0 / joined.shape[0])
    normed = (joined * lax.rsqrt(square + EPS) * gain_ref[...]).astype(bf16)
    out_ref[...] = lax.dot_general(
        normed, weight_ref[...], (((0,), (0,)), ((), ())), preferred_element_type=f32
    ).astype(bf16)
    for c in range(CS):
        log_ref[c : c + 1, :] = joined_rows(in_ref[c * XS + x_at[0], VD:, :])


def smem():
    return pl.BlockSpec(memory_space=pltpu.SMEM)


def vmem():
    return pl.BlockSpec(memory_space=pltpu.VMEM)


def call(kernel, out_shape, scalars, arrays, scratch=()):
    many = isinstance(out_shape, (tuple, list))
    return pl.pallas_call(
        kernel,
        out_shape=out_shape,
        in_specs=[smem()] * len(scalars) + [vmem()] * len(arrays),
        out_specs=[vmem() for _ in out_shape] if many else vmem(),
        scratch_shapes=list(scratch),
        compiler_params=pltpu.CompilerParams(vmem_limit_bytes=32 * 1024 * 1024),
    )(*scalars, *arrays)


def per_device(
    tokens,
    doc_lengths,
    query_down,
    latent_down,
    rope_down,
    query_latent_gain,
    latent_gain,
    query_up,
    key_up,
    value_up,
    query_gain,
    key_gain,
    output_gain,
    output_weight,
):
    z_at, y_at, c_at, x_at = (lax.axis_index(a) for a in ("z", "y", "c", "x"))
    query_latent = norm_rows(
        jnp.dot(tokens, query_down, preferred_element_type=f32), query_latent_gain
    ).astype(bf16)
    key_latent = norm_rows(
        jnp.dot(tokens, latent_down, preferred_element_type=f32), latent_gain
    ).astype(bf16)
    rope_key = jnp.dot(tokens, rope_down, preferred_element_type=f32).astype(bf16)
    rank_q, rank_k = query_latent.shape[1], key_latent.shape[1]
    every = spread(jnp.concatenate([query_latent, key_latent, rope_key], axis=1), ("x",))
    every = every.reshape(ROWS, -1)
    query_rows = every[:, :rank_q]
    latent_rows = every[:, rank_q : rank_q + rank_k]
    rope_rows = every[:, rank_q + rank_k :]

    offset = ((z_at * YS + y_at) * CS + c_at) * ROWS
    places = offset + jnp.arange(ROWS, dtype=jnp.int32)
    inverse = THETA ** (-jnp.arange(HALF, dtype=f32) / HALF)
    angles = places.astype(f32)[None, :] * inverse[:, None]
    cosine, sine = jnp.cos(angles), jnp.sin(angles)

    kv_out = call(
        kv_kernel,
        jax.ShapeDtypeStruct((ZS * CS, KV, ROWS), bf16),
        (),
        (latent_rows, rope_rows, key_up, value_up, key_gain[:, None], cosine, sine),
    )
    kv_all = lax.all_to_all(kv_out, ("z", "c"), split_axis=0, concat_axis=0, tiled=True)
    q_out = call(
        q_kernel,
        jax.ShapeDtypeStruct((CS * HW, ROWS), bf16),
        (),
        (query_rows, query_up, query_gain[:, None], cosine, sine),
    )
    q_all = lax.all_gather(q_out, ("y", "c"), axis=0)

    parts = call(
        attend_kernel,
        jax.ShapeDtypeStruct((YS, MSG, QB), bf16),
        (doc_lengths,),
        (q_all, kv_all),
        scratch=(
            pltpu.VMEM((ZS * KB, 128), bf16),
            pltpu.VMEM((YS, 128, QB), bf16),
            pltpu.VMEM((YS, 1, QB), f32),
            pltpu.VMEM((YS, 1, QB), f32),
            pltpu.VMEM((YS, VD, QB), f32),
        ),
    )
    parts = lax.all_to_all(parts, "y", split_axis=0, concat_axis=0, tiled=True)
    heads = call(combine_kernel, jax.ShapeDtypeStruct((CS * XS, MSG, ROWS), bf16), (), (parts,))
    heads = lax.all_to_all(heads, ("c", "x"), split_axis=0, concat_axis=0, tiled=True)
    layer_output, log_totals = call(
        output_kernel,
        (
            jax.ShapeDtypeStruct((ROWS, output_weight.shape[1]), bf16),
            jax.ShapeDtypeStruct((CS, ROWS), f32),
        ),
        (x_at.astype(jnp.int32).reshape(1),),
        (heads, output_gain[:, None], output_weight),
    )
    return (layer_output, log_totals)


def solution(mesh):
    fine = Mesh(mesh.devices.reshape(ZS, YS, CS, XS), ("z", "y", "c", "x"))
    sp = ("z", "y", "c")

    return jax.shard_map(
        per_device,
        mesh=fine,
        in_specs=(
            P((*sp, "x"), None),
            P(),
            P(),
            P(),
            P(),
            P(),
            P(),
            P(None, "x"),
            P(None, "x"),
            P(None, "x"),
            P(),
            P(),
            P(),
            P(None, "x"),
        ),
        out_specs=(P(sp, "x"), P("x", sp)),
        check_vma=False,
    )
```

profile of v0, /device:TPU:65, one launch (start us, length us, event | category | flops | bytes accessed | tf_op | source)
XLA Modules:
  0.0 95.1 jit_solution(3204883732578964627)
XLA Ops:
  0.6 0.0 copy-start
  0.6 0.0 copy-start.5
  0.7 0.0 copy-start.6
  0.7 0.0 copy-start.8
  0.7 0.0 copy-start.10
  0.7 0.0 copy-start.11
  0.7 0.0 copy-start.12
  0.7 0.0 copy-start.2
  0.7 0.0 copy-start.3
  0.7 1.5 %copy-done = bf16[2048,512]{1,0:T(8,128)(2,1)S(1)} copy-done((bf16[2048,512]{1,0:T(8,128)(2,1)S(1)}, bf16[2048,512]{1,0:T(8,128)(2,1)}, u32[]{:S(2)}) %copy-start) | copy-done | bytes 2097176
  2.2 1.5 %multiply_reduce_fusion = (f32[32]{0:T(128)S(1)}, f32[32,512]{1,0:T(8,128)S(1)}) fusion(bf16[32,2048]{1,0:T(8,128)(2,1)} %param.14, bf16[2048,512]{1,0:T(8,128)(2,1)S(1)} %copy-done), kind=kOutput, calls=%fused_computation.2 | convolution fusion | flops 67141600 | bytes 2293888 | tf_op jit(solution)/shard_map/dot_general | solution.py:271
  3.7 0.0 copy-done.5
  3.7 0.0 copy-done.6
  3.7 0.4 multiply_reduce_fusion.1
  4.1 0.0 copy-start.7
  4.2 0.0 copy-done.8
  4.2 0.0 copy-start.13
  4.2 0.2 convolution_convert_fusion
  4.3 0.0 copy-done.10
  4.4 0.1 multiply_convert_fusion
  4.4 0.0 copy-done.11
  4.4 0.1 multiply_convert_fusion.1
  4.5 0.7 broadcast_in_dim.8
  5.2 4.0 %all-to-all-start = ((bf16[4,32,800]{2,1,0:T(8,128)(2,1)}), bf16[4,32,800]{2,1,0:T(8,128)(2,1)S(1)}, u32[]{:S(2)}, u32[]{:S(2)}) async-start(bf16[4,32,800]{2,1,0:T(8,128)(2,1)} %broadcast_in_dim.8), calls=%async_computation | async-start | bytes 458752 | tf_op jit(solution)/shard_map/all_to_all | solution.py:44
  9.3 0.0 copy-done.12
  9.3 0.1 copy.21.gain_ref
  9.4 0.1 multiply_sine_fusion
  9.5 5.1 %all-to-all-done = bf16[4,32,800]{2,1,0:T(8,128)(2,1)S(1)} async-done(((bf16[4,32,800]{2,1,0:T(8,128)(2,1)}), bf16[4,32,800]{2,1,0:T(8,128)(2,1)S(1)}, u32[]{:S(2)}, u32[]{:S(2)}) %all-to-all-start) | async-done | bytes 204832 | tf_op jit(solution)/shard_map/all_to_all | solution.py:44
  14.6 0.0 copy-done.2
  14.6 0.0 copy-start.4
  14.7 1.1 %shard_map.150 = bf16[16,160,128]{2,1,0:T(8,128)(2,1)} custom-call(bf16[128,256]{1,0:T(8,128)(2,1)S(1)} %slice.13.lat_ref, bf16[128,32]{1,0:T(8,128)(2,1)S(1)} %slice.14.rope_ref, bf16[256,128]{1,0:T(8,128)(2,1)S(1)} %copy-done.2, bf16[256,128]{1,0:T(8,128)(2,1)S(1)} %copy-done.3, f32[96,1]{1,0:T(8,128)S(1)} %copy.21.gain_ref, ...), custom_call_target="tpu_custom_call" | custom-call | tf_op jit(solution)/shard_map/pallas_call | solution.py:243
  15.7 11.7 %all-to-all-start.1 = ((bf16[16,160,128]{2,1,0:T(8,128)(2,1)}), bf16[16,160,128]{2,1,0:T(8,128)(2,1)S(1)}, u32[]{:S(2)}, u32[]{:S(2)}) async-start(bf16[16,160,128]{2,1,0:T(8,128)(2,1)} %shard_map.150), calls=%async_computation.1 | async-start | bytes 1310720 | tf_op jit(solution)/shard_map/all_to_all | solution.py:296
  27.4 0.1 copy.19.query_up_ref
  27.6 0.0 copy-done.13
  27.6 0.1 copy.20.gain_ref
  27.7 0.3 shard_map.149
  28.0 0.0 copy-start.9
  28.0 20.0 %all-gather = bf16[3072,128]{1,0:T(8,128)(2,1)S(1)} all-gather(bf16[192,128]{1,0:T(8,128)(2,1)S(1)} %shard_map.149), channel_id=2, replica_groups=mesh['z'=8,'y'=8,'c'=2,'x'=4] {'y','c'}, dimensions={0}, use_global_device_ids=true | all-gather | bytes 835584 | tf_op jit(solution)/shard_map/all_gather | solution.py:303
  48.0 0.0 all-to-all-done.1.kv_ref
  48.0 0.0 copy-done.4
  48.0 15.7 %shard_map.151 = bf16[8,80,256]{2,1,0:T(8,128)(2,1)S(1)} custom-call(s32[16]{0:T(128)S(1)} %copy-done.4, bf16[16,192,128]{2,1,0:T(8,128)(2,1)S(1)} %bitcast.12, bf16[16,160,128]{2,1,0:T(8,128)(2,1)S(1)} %all-to-all-done.1.kv_ref), custom_call_target="tpu_custom_call" | custom-call | tf_op jit(solution)/shard_map/pallas_call | solution.py:243
  63.7 0.0 copy-start.1
  63.7 19.6 %all_to_all.20.in_ref = bf16[8,80,256]{2,1,0:T(8,128)(2,1)S(1)} all-to-all(bf16[8,80,256]{2,1,0:T(8,128)(2,1)S(1)} %shard_map.151), channel_id=1, replica_groups=mesh['z'=8,'y'=8,'c'=2,'x'=4] {'y'}, dimensions={0} | all-to-all | bytes 655360 | tf_op jit(solution)/shard_map/all_to_all | solution.py:318
  83.3 0.8 shard_map.152
  84.1 4.4 %all-to-all-start.3 = ((bf16[8,80,128]{2,1,0:T(8,128)(2,1)}), bf16[8,80,128]{2,1,0:T(8,128)(2,1)S(1)}, u32[]{:S(2)}, u32[]{:S(2)}) async-start(bf16[8,80,128]{2,1,0:T(8,128)(2,1)} %shard_map.152), calls=%async_computation.3 | async-start | bytes 327680 | tf_op jit(solution)/shard_map/all_to_all | solution.py:320
  88.6 0.1 copy.22.gain_ref
  88.7 5.3 %all-to-all-done.3.in_ref = bf16[8,80,128]{2,1,0:T(8,128)(2,1)S(1)} async-done(((bf16[8,80,128]{2,1,0:T(8,128)(2,1)}), bf16[8,80,128]{2,1,0:T(8,128)(2,1)S(1)}, u32[]{:S(2)}, u32[]{:S(2)}) %all-to-all-start.3) | async-done | bytes 163872 | tf_op jit(solution)/shard_map/all_to_all | solution.py:320
  94.1 1.0 %shard_map.153 = (bf16[128,512]{1,0:T(8,128)(2,1)}, f32[2,128]{1,0:T(2,128)}) custom-call(s32[1]{0:T(128)} %bitcast.x_at, bf16[8,80,128]{2,1,0:T(8,128)(2,1)S(1)} %all-to-all-done.3.in_ref, f32[512,1]{1,0:T(8,128)S(1)} %copy.22.gain_ref, bf16[512,512]{1,0:T(8,128)(2,1)S(1)} %copy-done.1), custom_call_target="tpu_custom_call" | custom-call | tf_op jit(solution)/shard_map/pallas_call | solution.py:243
  (12 shorter events, 0.1 us)
Async XLA Ops:
  0.6 1.6 %copy-start = (bf16[2048,512]{1,0:T(8,128)(2,1)S(1)}, bf16[2048,512]{1,0:T(8,128)(2,1)}, u32[]{:S(2)}) copy-start(bf16[2048,512]{1,0:T(8,128)(2,1)} %param.16) | copy-start | bytes 6291460
  0.6 3.1 %copy-start.5 = (bf16[32,2048]{1,0:T(8,128)(2,1)S(1)}, bf16[32,2048]{1,0:T(8,128)(2,1)}, u32[]{:S(2)}) copy-start(bf16[32,2048]{1,0:T(8,128)(2,1)} %param.14) | copy-start | bytes 393220
  0.7 3.1 %copy-start.6 = (bf16[2048,256]{1,0:T(8,128)(2,1)S(1)}, bf16[2048,256]{1,0:T(8,128)(2,1)}, u32[]{:S(2)}) copy-start(bf16[2048,256]{1,0:T(8,128)(2,1)} %param.17) | copy-start | bytes 3145732
  0.7 3.5 %copy-start.8 = (bf16[2048,32]{0,1:T(8,128)(2,1)S(1)}, bf16[2048,32]{0,1:T(8,128)(2,1)}, u32[]{:S(2)}) copy-start(bf16[2048,32]{0,1:T(8,128)(2,1)} %param.18) | copy-start | bytes 393220
  0.7 3.7 %copy-start.10 = (f32[512]{0:T(512)S(1)}, f32[512]{0:T(512)}, u32[]{:S(2)}) copy-start(f32[512]{0:T(512)} %param.19) | copy-start | bytes 6148
  0.7 3.7 %copy-start.11 = (f32[256]{0:T(256)S(1)}, f32[256]{0:T(256)}, u32[]{:S(2)}) copy-start(f32[256]{0:T(256)} %param.20) | copy-start | bytes 3076
  0.7 8.6 %copy-start.12 = (f32[96]{0:T(128)S(1)}, f32[96]{0:T(128)}, u32[]{:S(2)}) copy-start(f32[96]{0:T(128)} %param.25) | copy-start | bytes 1156
  0.7 13.9 %copy-start.2 = (bf16[256,128]{1,0:T(8,128)(2,1)S(1)}, bf16[256,128]{1,0:T(8,128)(2,1)}, u32[]{:S(2)}) copy-start(bf16[256,128]{1,0:T(8,128)(2,1)} %key_up_ref.1) | copy-start | bytes 196612
  0.7 13.9 %copy-start.3 = (bf16[256,128]{1,0:T(8,128)(2,1)S(1)}, bf16[256,128]{1,0:T(8,128)(2,1)}, u32[]{:S(2)}) copy-start(bf16[256,128]{1,0:T(8,128)(2,1)} %value_up_ref.1) | copy-start | bytes 196612
  4.1 23.3 %copy-start.7 = (bf16[512,192]{0,1:T(8,128)(2,1)S(1)}, bf16[512,192]{0,1:T(8,128)(2,1)}, u32[]{:S(2)}) copy-start(bf16[512,192]{0,1:T(8,128)(2,1)} %param.21) | copy-start | bytes 589828
  4.2 23.4 %copy-start.13 = (f32[96]{0:T(128)S(1)}, f32[96]{0:T(128)}, u32[]{:S(2)}) copy-start(f32[96]{0:T(128)} %param.24) | copy-start | bytes 1156
  5.2 9.4 %all-to-all-start = ((bf16[4,32,800]{2,1,0:T(8,128)(2,1)}), bf16[4,32,800]{2,1,0:T(8,128)(2,1)S(1)}, u32[]{:S(2)}, u32[]{:S(2)}) async-start(bf16[4,32,800]{2,1,0:T(8,128)(2,1)} %broadcast_in_dim.8), calls=%async_computation | async-start | bytes 458752 | tf_op jit(solution)/shard_map/all_to_all | solution.py:44
  14.6 33.3 %copy-start.4 = (s32[16]{0:T(128)S(1)}, s32[16]{0:T(128)}, u32[]{:S(2)}) copy-start(s32[16]{0:T(128)} %lengths.1) | copy-start | bytes 196
  15.7 32.2 %all-to-all-start.1 = ((bf16[16,160,128]{2,1,0:T(8,128)(2,1)}), bf16[16,160,128]{2,1,0:T(8,128)(2,1)S(1)}, u32[]{:S(2)}, u32[]{:S(2)}) async-start(bf16[16,160,128]{2,1,0:T(8,128)(2,1)} %shard_map.150), calls=%async_computation.1 | async-start | bytes 1310720 | tf_op jit(solution)/shard_map/all_to_all | solution.py:296
  28.0 60.6 %copy-start.9 = (f32[512]{0:T(512)S(1)}, f32[512]{0:T(512)}, u32[]{:S(2)}) copy-start(f32[512]{0:T(512)} %param.26) | copy-start | bytes 6148
  63.7 30.4 %copy-start.1 = (bf16[512,512]{1,0:T(8,128)(2,1)S(1)}, bf16[512,512]{1,0:T(8,128)(2,1)}, u32[]{:S(2)}) copy-start(bf16[512,512]{1,0:T(8,128)(2,1)} %weight_ref.1) | copy-start | bytes 1572868
  84.1 9.9 %all-to-all-start.3 = ((bf16[8,80,128]{2,1,0:T(8,128)(2,1)}), bf16[8,80,128]{2,1,0:T(8,128)(2,1)S(1)}, u32[]{:S(2)}, u32[]{:S(2)}) async-start(bf16[8,80,128]{2,1,0:T(8,128)(2,1)} %shard_map.152), calls=%async_computation.3 | async-start | bytes 327680 | tf_op jit(solution)/shard_map/all_to_all | solution.py:320
where the time goes:
time: 95.5 us; the launch traced here: 95.1 us
  blocking collectives  39.6 us (41%)
  starting transfers between devices  20.1 us (21%)
  Pallas kernels  18.9 us (20%)
  waiting for transfers between devices  10.4 us (11%)
  local copies, waits for them, and re-layouts  2.79 us (3%)
  matrix products  2.01 us (2%)
    all_gather x1, blocking collectives, per_device(): q_all = lax.all_gather(q_out, ('y', 'c'), axis=0)  20 us
    all_to_all x1, blocking collectives, per_device(): parts = lax.all_to_all(parts, 'y', split_axis=0, concat_axis=0, tiled=True)  19.6 us
    pallas_call x5, Pallas kernels, call(): pl.pallas_call(kernel, out_shape=out_shape, in_specs=[smem()] * len(scala...  18.9 us
    all_to_all x1, starting transfers between devices, per_device(): lax.all_to_all(kv_out, ('z', 'c'), split_axis=0, concat_axis=0, tiled=True)  11.7 us
    all_to_all x1, waiting for transfers between devices, per_device(): lax.all_to_all(heads, ('c', 'x'), split_axis=0, concat_axis=0, tiled=True)  5.34 us
    all_to_all x1, waiting for transfers between devices, spread(): return lax.all_to_all(copies, axes, split_axis=0, concat_axis=0, tiled=True)  5.09 us
    all_to_all x1, starting transfers between devices, per_device(): lax.all_to_all(heads, ('c', 'x'), split_axis=0, concat_axis=0, tiled=True)  4.44 us
    all_to_all x1, starting transfers between devices, spread(): return lax.all_to_all(copies, axes, split_axis=0, concat_axis=0, tiled=True)  4.01 us
  transfers between devices with their start and end apart: 3, of which 2 were waited for; matrix products, arithmetic and copies ran while one was open for 1% of the time, Pallas kernels for 0%

commit v1 on v0

--- a/solution.py
+++ b/solution.py
@@ -106,8 +106,8 @@
     return (rows[0:1] + rows[1:2]) + rows[2:3]
 
 
-SUB = 2
 DOCS = 16
+SLAB = 16
 PAD = 128 - HW
 
 
@@ -152,41 +152,56 @@
     l_s[...] = jnp.zeros(l_s.shape, f32)
     acc_s[...] = jnp.zeros(acc_s.shape, f32)
 
-    def block(t, j):
-        keys = k_s[pl.ds(j * KB, KB), :]
-        values = jnp.concatenate([kv_ref[2 * j, HW:, :], kv_ref[2 * j + 1, HW:, :]], axis=1)
-        for s in range(SUB):
-            at = t * SUB + s
-            scores = jnp.dot(keys, q_s[at], preferred_element_type=f32)
-            before = m_s[at]
-            now = jnp.maximum(before, jnp.max(scores, axis=0, keepdims=True))
-            weights = jnp.exp2((scores - now) * SCALE2)
-            rescale = jnp.exp2((before - now) * SCALE2)
-            m_s[at] = now
-            l_s[at] = l_s[at] * rescale + jnp.sum(weights, axis=0, keepdims=True)
-            acc_s[at] = acc_s[at] * rescale + jnp.dot(
-                values, weights.astype(bf16), preferred_element_type=f32
-            )
-
-    def query_step(t, _):
-        begin = query_base + t * (SUB * QB)
-        first = doc_of(begin, ends)
-        last = doc_of(begin + (SUB * QB - 1), ends)
-
-        def key_step(j, _):
-            start = key_base + j * (YS * QB)
-            least = doc_of(start, ends)
-            most = doc_of(start + (KB - 1), ends)
-
-            @pl.when((least <= last) & (most >= first))
-            def _():
-                block(t, j)
-
-            return 0
-
-        return lax.fori_loop(0, ZS, key_step, 0)
-
-    lax.fori_loop(0, YS // SUB, query_step, 0)
+    first = doc_of(query_base, ends)
+    last = doc_of(query_base + (YS * QB - 1), ends)
+
+    def key_step(j, _):
+        start = key_base + j * (YS * QB)
+        least = doc_of(start, ends)
+        most = doc_of(start + (KB - 1), ends)
+
+        @pl.when((least <= last) & (most >= first))
+        def _():
+            keys = k_s[pl.ds(pl.multiple_of(j * KB, KB), KB), :]
+            values = jnp.concatenate([kv_ref[2 * j, HW:, :], kv_ref[2 * j + 1, HW:, :]], axis=1)
+            ahead = jnp.dot(keys, q_s[0], preferred_element_type=f32)
+            peak = jnp.max(ahead, axis=0, keepdims=True)
+            waiting = None
+            for at in range(YS):
+                scores = ahead
+                before = m_s[at]
+                now = jnp.maximum(before, peak)
+                rescale = jnp.exp2((before - now) * SCALE2)
+                m_s[at] = now
+                if at + 1 < YS:
+                    ahead = jnp.dot(keys, q_s[at + 1], preferred_element_type=f32)
+                    peaks = jnp.full((8, QB), START, f32)
+                sums = jnp.zeros((8, QB), f32)
+                pieces = []
+                for r in range(0, KB, SLAB):
+                    w = jnp.exp2((scores[r : r + SLAB] - now) * SCALE2)
+                    for i in range(0, SLAB, 8):
+                        sums = sums + w[i : i + 8]
+                    pieces.append(w.astype(bf16))
+                    if at + 1 < YS:
+                        for i in range(r, r + SLAB, 8):
+                            peaks = jnp.maximum(peaks, ahead[i : i + 8])
+                if waiting is not None:
+                    was, scaled, product = waiting
+                    acc_s[was] = acc_s[was] * scaled + product
+                product = jnp.dot(
+                    values, jnp.concatenate(pieces, axis=0), preferred_element_type=f32
+                )
+                waiting = (at, rescale, product)
+                l_s[at] = l_s[at] * rescale + jnp.sum(sums, axis=0, keepdims=True)
+                if at + 1 < YS:
+                    peak = jnp.max(peaks, axis=0, keepdims=True)
+            was, scaled, product = waiting
+            acc_s[was] = acc_s[was] * scaled + product
+
+        return 0
+
+    lax.fori_loop(0, ZS, key_step, 0)
     for i in range(YS):
         total = l_s[i]
         some = total > 0.0

time: 95.5 us -> 88.1 us (0.923)
  the two profiles are of different devices: /device:TPU:65 before, /device:TPU:1 now
where the time goes in v1:
time: 88.1 us; the launch traced here: 87.6 us
  blocking collectives  38.8 us (44%)
  starting transfers between devices  20.6 us (23%)
  Pallas kernels  12.5 us (14%)
  waiting for transfers between devices  9.62 us (11%)
  local copies, waits for them, and re-layouts  2.8 us (3%)
  matrix products  2.01 us (2%)
  between operations  0.92 us (1%)
    all_gather x1, blocking collectives, per_device(): q_all = lax.all_gather(q_out, ('y', 'c'), axis=0)  19.7 us
    all_to_all x1, blocking collectives, per_device(): parts = lax.all_to_all(parts, 'y', split_axis=0, concat_axis=0, tiled=True)  19.1 us
    pallas_call x5, Pallas kernels, call(): pl.pallas_call(kernel, out_shape=out_shape, in_specs=[smem()] * len(scala...  12.5 us
    all_to_all x1, starting transfers between devices, per_device(): lax.all_to_all(kv_out, ('z', 'c'), split_axis=0, concat_axis=0, tiled=True)  12.4 us
    all_to_all x1, waiting for transfers between devices, spread(): return lax.all_to_all(copies, axes, split_axis=0, concat_axis=0, tiled=True)  5.09 us
    all_to_all x1, starting transfers between devices, spread(): return lax.all_to_all(copies, axes, split_axis=0, concat_axis=0, tiled=True)  4.83 us
    all_to_all x1, waiting for transfers between devices, per_device(): lax.all_to_all(heads, ('c', 'x'), split_axis=0, concat_axis=0, tiled=True)  4.53 us
    all_to_all x1, starting transfers between devices, per_device(): lax.all_to_all(heads, ('c', 'x'), split_axis=0, concat_axis=0, tiled=True)  3.33 us
  transfers between devices with their start and end apart: 3, of which 2 were waited for; matrix products, arithmetic and copies ran while one was open for 1% of the time, Pallas kernels for 0%

profile of v1, /device:TPU:1, one launch (start us, length us, event | category | flops | bytes accessed | tf_op | source)
XLA Modules:
  0.0 87.6 jit_solution(5159101518321843076)
XLA Ops:
  0.6 0.0 copy-start
  0.6 0.0 copy-start.5
  0.7 0.0 copy-start.6
  0.7 0.0 copy-start.8
  0.7 0.0 copy-start.10
  0.7 0.0 copy-start.11
  0.7 0.0 copy-start.12
  0.7 0.0 copy-start.2
  0.7 0.0 copy-start.3
  0.7 1.5 %copy-done = bf16[2048,512]{1,0:T(8,128)(2,1)S(1)} copy-done((bf16[2048,512]{1,0:T(8,128)(2,1)S(1)}, bf16[2048,512]{1,0:T(8,128)(2,1)}, u32[]{:S(2)}) %copy-start) | copy-done | bytes 2097176
  2.2 1.5 %multiply_reduce_fusion = (f32[32]{0:T(128)S(1)}, f32[32,512]{1,0:T(8,128)S(1)}) fusion(bf16[32,2048]{1,0:T(8,128)(2,1)} %param.14, bf16[2048,512]{1,0:T(8,128)(2,1)S(1)} %copy-done), kind=kOutput, calls=%fused_computation.2 | convolution fusion | flops 67141600 | bytes 2293888 | tf_op jit(solution)/shard_map/dot_general | solution.py:286
  3.7 0.0 copy-done.5
  3.7 0.0 copy-done.6
  3.7 0.4 multiply_reduce_fusion.1
  4.1 0.0 copy-start.7
  4.2 0.0 copy-done.8
  4.2 0.0 copy-start.13
  4.2 0.2 convolution_convert_fusion
  4.3 0.0 copy-done.10
  4.4 0.1 multiply_convert_fusion
  4.4 0.0 copy-done.11
  4.4 0.1 multiply_convert_fusion.1
  4.5 0.7 broadcast_in_dim.8
  5.2 4.8 %all-to-all-start = ((bf16[4,32,800]{2,1,0:T(8,128)(2,1)}), bf16[4,32,800]{2,1,0:T(8,128)(2,1)S(1)}, u32[]{:S(2)}, u32[]{:S(2)}) async-start(bf16[4,32,800]{2,1,0:T(8,128)(2,1)} %broadcast_in_dim.8), calls=%async_computation | async-start | bytes 458752 | tf_op jit(solution)/shard_map/all_to_all | solution.py:44
  10.1 0.0 copy-done.12
  10.1 0.1 copy.21.gain_ref
  10.2 0.1 multiply_sine_fusion
  10.3 5.1 %all-to-all-done = bf16[4,32,800]{2,1,0:T(8,128)(2,1)S(1)} async-done(((bf16[4,32,800]{2,1,0:T(8,128)(2,1)}), bf16[4,32,800]{2,1,0:T(8,128)(2,1)S(1)}, u32[]{:S(2)}, u32[]{:S(2)}) %all-to-all-start) | async-done | bytes 204832 | tf_op jit(solution)/shard_map/all_to_all | solution.py:44
  15.4 0.0 copy-done.2
  15.4 0.0 copy-done.3
  15.4 0.0 copy-start.4
  15.5 1.1 %shard_map.150 = bf16[16,160,128]{2,1,0:T(8,128)(2,1)} custom-call(bf16[128,256]{1,0:T(8,128)(2,1)S(1)} %slice.13.lat_ref, bf16[128,32]{1,0:T(8,128)(2,1)S(1)} %slice.14.rope_ref, bf16[256,128]{1,0:T(8,128)(2,1)S(1)} %copy-done.2, bf16[256,128]{1,0:T(8,128)(2,1)S(1)} %copy-done.3, f32[96,1]{1,0:T(8,128)S(1)} %copy.21.gain_ref, ...), custom_call_target="tpu_custom_call" | custom-call | tf_op jit(solution)/shard_map/pallas_call | solution.py:258
  16.6 12.4 %all-to-all-start.1 = ((bf16[16,160,128]{2,1,0:T(8,128)(2,1)}), bf16[16,160,128]{2,1,0:T(8,128)(2,1)S(1)}, u32[]{:S(2)}, u32[]{:S(2)}) async-start(bf16[16,160,128]{2,1,0:T(8,128)(2,1)} %shard_map.150), calls=%async_computation.1 | async-start | bytes 1310720 | tf_op jit(solution)/shard_map/all_to_all | solution.py:311
  29.0 0.0 copy-done.7
  29.0 0.1 copy.19.query_up_ref
  29.1 0.1 copy.20.gain_ref
  29.3 0.3 shard_map.149
  29.5 0.0 copy-start.9
  29.6 19.7 %all-gather = bf16[3072,128]{1,0:T(8,128)(2,1)S(1)} all-gather(bf16[192,128]{1,0:T(8,128)(2,1)S(1)} %shard_map.149), channel_id=2, replica_groups=mesh['z'=8,'y'=8,'c'=2,'x'=4] {'y','c'}, dimensions={0}, use_global_device_ids=true | all-gather | bytes 835584 | tf_op jit(solution)/shard_map/all_gather | solution.py:318
  49.2 0.0 all-to-all-done.1.kv_ref
  49.2 9.4 %shard_map.151 = bf16[8,80,256]{2,1,0:T(8,128)(2,1)S(1)} custom-call(s32[16]{0:T(128)S(1)} %copy-done.4, bf16[16,192,128]{2,1,0:T(8,128)(2,1)S(1)} %bitcast.12, bf16[16,160,128]{2,1,0:T(8,128)(2,1)S(1)} %all-to-all-done.1.kv_ref), custom_call_target="tpu_custom_call" | custom-call | tf_op jit(solution)/shard_map/pallas_call | solution.py:258
  58.6 0.0 copy-start.1
  58.6 19.1 %all_to_all.20.in_ref = bf16[8,80,256]{2,1,0:T(8,128)(2,1)S(1)} all-to-all(bf16[8,80,256]{2,1,0:T(8,128)(2,1)S(1)} %shard_map.151), channel_id=1, replica_groups=mesh['z'=8,'y'=8,'c'=2,'x'=4] {'y'}, dimensions={0} | all-to-all | bytes 655360 | tf_op jit(solution)/shard_map/all_to_all | solution.py:333
  77.8 0.8 shard_map.152
  78.6 3.3 %all-to-all-start.3 = ((bf16[8,80,128]{2,1,0:T(8,128)(2,1)}), bf16[8,80,128]{2,1,0:T(8,128)(2,1)S(1)}, u32[]{:S(2)}, u32[]{:S(2)}) async-start(bf16[8,80,128]{2,1,0:T(8,128)(2,1)} %shard_map.152), calls=%async_computation.3 | async-start | bytes 327680 | tf_op jit(solution)/shard_map/all_to_all | solution.py:335
  81.9 0.1 copy.22.gain_ref
  82.1 4.5 %all-to-all-done.3.in_ref = bf16[8,80,128]{2,1,0:T(8,128)(2,1)S(1)} async-done(((bf16[8,80,128]{2,1,0:T(8,128)(2,1)}), bf16[8,80,128]{2,1,0:T(8,128)(2,1)S(1)}, u32[]{:S(2)}, u32[]{:S(2)}) %all-to-all-start.3) | async-done | bytes 163872 | tf_op jit(solution)/shard_map/all_to_all | solution.py:335
  86.6 1.0 %shard_map.153 = (bf16[128,512]{1,0:T(8,128)(2,1)}, f32[2,128]{1,0:T(2,128)}) custom-call(s32[1]{0:T(128)} %bitcast.x_at, bf16[8,80,128]{2,1,0:T(8,128)(2,1)S(1)} %all-to-all-done.3.in_ref, f32[512,1]{1,0:T(8,128)S(1)} %copy.22.gain_ref, bf16[512,512]{1,0:T(8,128)(2,1)S(1)} %copy-done.1), custom_call_target="tpu_custom_call" | custom-call | tf_op jit(solution)/shard_map/pallas_call | solution.py:258
  (12 shorter events, 0.1 us)
Async XLA Ops:
  0.6 1.6 %copy-start = (bf16[2048,512]{1,0:T(8,128)(2,1)S(1)}, bf16[2048,512]{1,0:T(8,128)(2,1)}, u32[]{:S(2)}) copy-start(bf16[2048,512]{1,0:T(8,128)(2,1)} %param.16) | copy-start | bytes 6291460
  0.6 3.1 %copy-start.5 = (bf16[32,2048]{1,0:T(8,128)(2,1)S(1)}, bf16[32,2048]{1,0:T(8,128)(2,1)}, u32[]{:S(2)}) copy-start(bf16[32,2048]{1,0:T(8,128)(2,1)} %param.14) | copy-start | bytes 393220
  0.7 3.1 %copy-start.6 = (bf16[2048,256]{1,0:T(8,128)(2,1)S(1)}, bf16[2048,256]{1,0:T(8,128)(2,1)}, u32[]{:S(2)}) copy-start(bf16[2048,256]{1,0:T(8,128)(2,1)} %param.17) | copy-start | bytes 3145732
  0.7 3.5 %copy-start.8 = (bf16[2048,32]{0,1:T(8,128)(2,1)S(1)}, bf16[2048,32]{0,1:T(8,128)(2,1)}, u32[]{:S(2)}) copy-start(bf16[2048,32]{0,1:T(8,128)(2,1)} %param.18) | copy-start | bytes 393220
  0.7 3.7 %copy-start.10 = (f32[512]{0:T(512)S(1)}, f32[512]{0:T(512)}, u32[]{:S(2)}) copy-start(f32[512]{0:T(512)} %param.19) | copy-start | bytes 6148
  0.7 3.7 %copy-start.11 = (f32[256]{0:T(256)S(1)}, f32[256]{0:T(256)}, u32[]{:S(2)}) copy-start(f32[256]{0:T(256)} %param.20) | copy-start | bytes 3076
  0.7 9.4 %copy-start.12 = (f32[96]{0:T(128)S(1)}, f32[96]{0:T(128)}, u32[]{:S(2)}) copy-start(f32[96]{0:T(128)} %param.25) | copy-start | bytes 1156
  0.7 14.7 %copy-start.2 = (bf16[256,128]{1,0:T(8,128)(2,1)S(1)}, bf16[256,128]{1,0:T(8,128)(2,1)}, u32[]{:S(2)}) copy-start(bf16[256,128]{1,0:T(8,128)(2,1)} %key_up_ref.1) | copy-start | bytes 196612
  0.7 14.7 %copy-start.3 = (bf16[256,128]{1,0:T(8,128)(2,1)S(1)}, bf16[256,128]{1,0:T(8,128)(2,1)}, u32[]{:S(2)}) copy-start(bf16[256,128]{1,0:T(8,128)(2,1)} %value_up_ref.1) | copy-start | bytes 196612
  4.1 24.9 %copy-start.7 = (bf16[512,192]{0,1:T(8,128)(2,1)S(1)}, bf16[512,192]{0,1:T(8,128)(2,1)}, u32[]{:S(2)}) copy-start(bf16[512,192]{0,1:T(8,128)(2,1)} %param.21) | copy-start | bytes 589828
  4.2 25.0 %copy-start.13 = (f32[96]{0:T(128)S(1)}, f32[96]{0:T(128)}, u32[]{:S(2)}) copy-start(f32[96]{0:T(128)} %param.24) | copy-start | bytes 1156
  5.2 10.2 %all-to-all-start = ((bf16[4,32,800]{2,1,0:T(8,128)(2,1)}), bf16[4,32,800]{2,1,0:T(8,128)(2,1)S(1)}, u32[]{:S(2)}, u32[]{:S(2)}) async-start(bf16[4,32,800]{2,1,0:T(8,128)(2,1)} %broadcast_in_dim.8), calls=%async_computation | async-start | bytes 458752 | tf_op jit(solution)/shard_map/all_to_all | solution.py:44
  15.4 33.8 %copy-start.4 = (s32[16]{0:T(128)S(1)}, s32[16]{0:T(128)}, u32[]{:S(2)}) copy-start(s32[16]{0:T(128)} %lengths.1) | copy-start | bytes 196
  16.6 32.7 %all-to-all-start.1 = ((bf16[16,160,128]{2,1,0:T(8,128)(2,1)}), bf16[16,160,128]{2,1,0:T(8,128)(2,1)S(1)}, u32[]{:S(2)}, u32[]{:S(2)}) async-start(bf16[16,160,128]{2,1,0:T(8,128)(2,1)} %shard_map.150), calls=%async_computation.1 | async-start | bytes 1310720 | tf_op jit(solution)/shard_map/all_to_all | solution.py:311
  29.5 52.4 %copy-start.9 = (f32[512]{0:T(512)S(1)}, f32[512]{0:T(512)}, u32[]{:S(2)}) copy-start(f32[512]{0:T(512)} %param.26) | copy-start | bytes 6148
  58.6 28.0 %copy-start.1 = (bf16[512,512]{1,0:T(8,128)(2,1)S(1)}, bf16[512,512]{1,0:T(8,128)(2,1)}, u32[]{:S(2)}) copy-start(bf16[512,512]{1,0:T(8,128)(2,1)} %weight_ref.1) | copy-start | bytes 1572868
  78.6 8.0 %all-to-all-start.3 = ((bf16[8,80,128]{2,1,0:T(8,128)(2,1)}), bf16[8,80,128]{2,1,0:T(8,128)(2,1)S(1)}, u32[]{:S(2)}, u32[]{:S(2)}) async-start(bf16[8,80,128]{2,1,0:T(8,128)(2,1)} %shard_map.152), calls=%async_computation.3 | async-start | bytes 327680 | tf_op jit(solution)/shard_map/all_to_all | solution.py:335
